TPU v7x, 32 devices: a whole 2x2x4 slice. The times are simulated.
32 devices in a mesh: sp: 8 (over z, x), tp: 4 (over y, core).
Axes of the slice: x: 2, y: 2, z: 4, core: 2. Of those that a mesh axis runs over, the one named last changes fastest.
Arguments:
- stream: bfloat16 [4096, 2048], P('sp', 'tp'), may hold values from -6 to 6
- norm_gain: float32 [2, 2048], replicated, may hold values from 0.1 to 1.9
- w_value: bfloat16 [2, 2048, 2048], P(None, 'sp', 'tp'), may hold values from -0.125 to 0.125
- w_inner: bfloat16 [2, 2048, 2048], P(None, 'sp', 'tp'), may hold values from -0.125 to 0.125
- w_outer: bfloat16 [2, 2048, 2048], P(None, 'sp', 'tp'), may hold values from -0.125 to 0.125
- conv_taps: float32 [2, 3, 2048], P(None, None, 'tp'), may hold values from -3 to 3
- w_output: bfloat16 [2, 2048, 2048], P(None, 'tp', 'sp'), may hold values from -0.125 to 0.125
Outputs:
- result: bfloat16 [4096, 2048], P('sp', 'tp')
All inputs are finite; a program needn't handle non-finite values.
Results may differ from a plain program's by a relative error of at most 0.02.
Values may be sent and summed in bfloat16 or wider, within the bound.
A program may use at most 64 MiB of HBM per device.

v0:
```python
import jax
import jax.numpy as jnp
from jax import lax
from jax.sharding import PartitionSpec as P

LAYERS = 2
EPSILON = 1e-06


def passed_along(block, axis, distance):
    devices = range(lax.axis_size(axis))
    route = [(i - distance, i) for i in devices if i - distance in devices]
    return lax.ppermute(block, axis, route)


def on_device(stream, norm_gain, w_value, w_inner, w_outer, conv_taps, w_output):
    gathered_in = (
        lax.all_gather(w_value, "sp", axis=1, tiled=True),
        lax.all_gather(w_inner, "sp", axis=1, tiled=True),
        lax.all_gather(w_outer, "sp", axis=1, tiled=True),
    )
    gathered_out = lax.all_gather(w_output, "sp", axis=2, tiled=True)
    stream_now = stream
    for layer_index in range(LAYERS):
        layer_value = gathered_in[0][layer_index]
        layer_inner = gathered_in[1][layer_index]
        layer_outer = gathered_in[2][layer_index]
        layer_output = gathered_out[layer_index]
        full_rows = lax.all_gather(stream_now, "tp", axis=1, tiled=True)
        row_float = full_rows.astype(jnp.float32)
        scale = lax.rsqrt(jnp.mean(row_float * row_float, axis=-1, keepdims=True) + EPSILON)
        normed = (row_float * scale * norm_gain[layer_index]).astype(jnp.bfloat16)
        row_count = normed.shape[0]
        value_proj = jnp.dot(normed, layer_value, preferred_element_type=jnp.float32)
        inner_gate = jnp.dot(normed, layer_inner, preferred_element_type=jnp.float32)
        outer_gate = jnp.dot(normed, layer_outer, preferred_element_type=jnp.float32)
        mixed = (inner_gate * value_proj).astype(jnp.bfloat16)
        before = passed_along(mixed[row_count - 2 :], "sp", 1)
        padded = jnp.concatenate([before, mixed], axis=0).astype(jnp.float32)
        taps = conv_taps[layer_index]
        convolved = (
            taps[0] * padded[0:row_count]
            + taps[1] * padded[1 : row_count + 1]
            + taps[2] * padded[2:]
        )
        gated = (outer_gate * convolved).astype(jnp.bfloat16)
        terms = jnp.dot(gated, layer_output, preferred_element_type=jnp.float32).astype(
            jnp.bfloat16
        )
        summed = lax.psum_scatter(
            terms.astype(jnp.float32).astype(jnp.bfloat16), "tp", scatter_dimension=1, tiled=True
        ).astype(jnp.float32)
        stream_now = (stream_now.astype(jnp.float32) + summed).astype(jnp.bfloat16)
    return stream_now


def solution(mesh):
    in_specs = (
        P("sp", "tp"),
        P(),
        P(None, "sp", "tp"),
        P(None, "sp", "tp"),
        P(None, "sp", "tp"),
        P(None, None, "tp"),
        P(None, "tp", "sp"),
    )
    out_specs = P("sp", "tp")
    return jax.shard_map(
        on_device, mesh=mesh, in_specs=in_specs, out_specs=out_specs, check_vma=False
    )
```

profile of v0, /device:TPU:0, one launch (start us, length us, event | category | flops | bytes accessed | tf_op | source)
XLA Modules:
  0.0 450.2 jit_solution(300876081806969072)
XLA Ops:
  6.5 0.0 all-gather.7.cloned.1.call-start
  6.5 0.7 all-gather.7.cloned.1.call-update
  7.3 0.0 all-gather.13.cloned.1.call-start
  7.3 0.7 all-gather.13.cloned.1.call-update
  8.0 0.0 all-gather.11.cloned.1.call-start
  8.1 0.7 all-gather.11.cloned.1.call-update
  8.7 0.0 all-gather.9.cloned.1.call-start
  8.8 0.5 all-gather.9.cloned.1.call-update
  9.3 0.0 all-gather.15.cloned.1.call-start
  9.4 0.5 all-gather.15.cloned.1.call-update
  9.9 0.0 reduce-scatter.3.cloned.1.call-start
  10.0 0.0 copy-done.4
  10.0 24.2 %all-gather.7.cloned.1.call-done = bf16[512,2048]{1,0:T(8,128)(2,1)} async-done(((bf16[512,512]{1,0:T(8,128)(2,1)}), bf16[512,2048]{1,0:T(8,128)(2,1)}) %all-gather.7.cloned.1.call-update) | async-done | bytes 2097168 | tf_op jit(solution)/shard_map/all_gather | solution.py:29
  34.2 2.2 fusion
  36.5 72.7 %all-gather.13.cloned.1.call-done = bf16[2,2048,512]{2,1,0:T(8,128)(2,1)} async-done(((bf16[2,256,512]{2,1,0:T(8,128)(2,1)}), bf16[2,2048,512]{2,1,0:T(8,128)(2,1)}) %all-gather.13.cloned.1.call-update) | async-done | bytes 4194320 | tf_op jit(solution)/shard_map/all_gather | solution.py:18
  109.2 0.0 copy-done.2
  109.2 2.9 fusion.9
  112.1 0.0 copy-start.5
  112.1 70.6 %all-gather.11.cloned.1.call-done = bf16[2,2048,512]{2,1,0:T(8,128)(2,1)} async-done(((bf16[2,256,512]{2,1,0:T(8,128)(2,1)}), bf16[2,2048,512]{2,1,0:T(8,128)(2,1)}) %all-gather.11.cloned.1.call-update) | async-done | bytes 4194320 | tf_op jit(solution)/shard_map/all_gather | solution.py:19
  182.7 2.9 fusion.18
  185.6 2.5 collective-permute-start
  188.1 0.0 copy-done.5
  188.1 1.3 collective-permute-done
  189.4 0.2 maximum_convert_fusion
  189.6 66.6 %all-gather.9.cloned.1.call-done = bf16[2,2048,512]{2,1,0:T(8,128)(2,1)} async-done(((bf16[2,256,512]{2,1,0:T(8,128)(2,1)}), bf16[2,2048,512]{2,1,0:T(8,128)(2,1)}) %all-gather.9.cloned.1.call-update) | async-done | bytes 4194320 | tf_op jit(solution)/shard_map/all_gather | solution.py:20
  256.1 75.1 %all-gather.15.cloned.1.call-done = bf16[2,512,2048]{2,1,0:T(8,128)(2,1)} async-done(((bf16[2,512,256]{2,1,0:T(8,128)(2,1)}), bf16[2,512,2048]{2,1,0:T(8,128)(2,1)}) %all-gather.15.cloned.1.call-update) | async-done | bytes 4194320 | tf_op jit(solution)/shard_map/all_gather | solution.py:22
  331.2 6.1 %convolution_convert_fusion.1 = bf16[512,2048]{1,0:T(8,128)(2,1)} fusion(bf16[2,512,2048]{2,1,0:T(8,128)(2,1)} %all-gather.15.cloned.1.call-done, bf16[2,2048,512]{2,1,0:T(8,128)(2,1)} %all-gather.9.cloned.1.call-done, f32[514,512]{1,0:T(8,128)S(1)} %maximum_convert_fusion, f32[512]{0:T(512)S(1)} %bitcast.61, f32[512]{0:T(512)S(1)} %bitcast.62, ...), kind=kOutput, calls=%fused_computation.11 | convolution fusion | flops 2154561536 | bytes 11550720 | tf_op jit(solution)/shard_map/dot_general | solution.py:47
  337.3 0.0 reduce-scatter.3.cloned.1.call-update
  337.3 0.0 all-gather.17.cloned.1.call-start
  337.4 29.5 %reduce-scatter.3.cloned.1.call-done = bf16[512,512]{1,0:T(8,128)(2,1)} async-done(((bf16[512,2048]{1,0:T(8,128)(2,1)}), bf16[512,512]{1,0:T(8,128)(2,1)}) %reduce-scatter.3.cloned.1.call-update) | async-done | bytes 524304 | tf_op jit(solution)/shard_map/reduce_scatter | solution.py:50
  366.9 0.0 copy-done.1
  366.9 2.0 add_convert_fusion.1
  368.8 0.0 all-gather.17.cloned.1.call-update
  368.9 0.0 reduce-scatter.5.cloned.1.call-start
  368.9 22.6 %all-gather.17.cloned.1.call-done = bf16[512,2048]{1,0:T(8,128)(2,1)} async-done(((bf16[512,512]{1,0:T(8,128)(2,1)}), bf16[512,2048]{1,0:T(8,128)(2,1)}) %all-gather.17.cloned.1.call-update) | async-done | bytes 2097168 | tf_op jit(solution)/shard_map/all_gather | solution.py:29
  391.6 2.2 fusion.3
  393.8 0.0 copy-done.3
  393.8 0.0 copy-start.6
  393.8 3.0 fusion.6
  396.9 1.3 fusion.16
  398.2 3.4 collective-permute-start.1
  401.6 1.3 collective-permute-done.1
  402.8 0.2 maximum_convert_fusion.1
  403.0 6.2 %convolution_convert_fusion = bf16[512,2048]{1,0:T(8,128)(2,1)} fusion(bf16[2,512,2048]{2,1,0:T(8,128)(2,1)} %all-gather.15.cloned.1.call-done, bf16[2,2048,512]{2,1,0:T(8,128)(2,1)} %all-gather.9.cloned.1.call-done, f32[514,512]{1,0:T(8,128)S(1)} %maximum_convert_fusion.1, f32[512]{0:T(512)S(1)} %bitcast.59, f32[512]{0:T(512)S(1)} %bitcast.60, ...), kind=kOutput, calls=%fused_computation.10 | convolution fusion | flops 2154561536 | bytes 11550720 | tf_op jit(solution)/shard_map/dot_general | solution.py:47
  409.2 0.0 reduce-scatter.5.cloned.1.call-update
  409.2 32.1 %reduce-scatter.5.cloned.1.call-done = bf16[512,512]{1,0:T(8,128)(2,1)} async-done(((bf16[512,2048]{1,0:T(8,128)(2,1)}), bf16[512,512]{1,0:T(8,128)(2,1)}) %reduce-scatter.5.cloned.1.call-update) | async-done | bytes 524304 | tf_op jit(solution)/shard_map/reduce_scatter | solution.py:50
  441.4 0.0 copy-done
  441.4 2.0 add_convert_fusion
  (12 shorter events, 0.1 us)
Async XLA Ops:
  6.5 3.4 copy-start.4
  6.5 27.7 %all-gather.7.cloned.1.call-start = ((), (), s32[]{:S(2)}) async-start(), calls=%async_computation.2 | async-start | bytes 2621440 | tf_op jit(solution)/shard_map/all_gather | solution.py:29
  7.3 101.9 %all-gather.13.cloned.1.call-start = ((), (), s32[]{:S(2)}) async-start(), calls=%async_computation.5 | async-start | bytes 4718592 | tf_op jit(solution)/shard_map/all_gather | solution.py:18
  8.0 174.7 %all-gather.11.cloned.1.call-start = ((), (), s32[]{:S(2)}) async-start(), calls=%async_computation.4 | async-start | bytes 4718592 | tf_op jit(solution)/shard_map/all_gather | solution.py:19
  8.7 247.4 %all-gather.9.cloned.1.call-start = ((), (), s32[]{:S(2)}) async-start(), calls=%async_computation.3 | async-start | bytes 4718592 | tf_op jit(solution)/shard_map/all_gather | solution.py:20
  9.3 321.9 %all-gather.15.cloned.1.call-start = ((), (), s32[]{:S(2)}) async-start(), calls=%async_computation.6 | async-start | bytes 4718592 | tf_op jit(solution)/shard_map/all_gather | solution.py:22
  9.9 357.0 %reduce-scatter.3.cloned.1.call-start = ((), (), s32[]{:S(2)}) async-start(), calls=%async_computation.7 | async-start | bytes 2621440 | tf_op jit(solution)/shard_map/reduce_scatter | solution.py:50
  34.2 75.0 %copy-start.2 = (bf16[512,2048]{1,0:T(8,128)(2,1)S(1)}, bf16[512,2048]{1,0:T(8,128)(2,1)}, u32[]{:S(2)}) copy-start(bf16[512,2048]{1,0:T(8,128)(2,1)} %all-gather.7.cloned.1.call-done) | copy-start | bytes 6291460
  112.1 76.0 %copy-start.5 = (f32[2,3,512]{2,0,1:T(2,128)S(1)}, f32[2,3,512]{2,0,1:T(2,128)}, u32[]{:S(2)}) copy-start(f32[2,3,512]{2,0,1:T(2,128)} %param.12) | copy-start | bytes 36868
  185.6 3.8 collective-permute-start
  337.3 29.5 %copy-start.1 = (bf16[512,512]{1,0:T(8,128)(2,1)S(1)}, bf16[512,512]{1,0:T(8,128)(2,1)}, u32[]{:S(2)}) copy-start(bf16[512,512]{1,0:T(8,128)(2,1)} %param.7) | copy-start | bytes 1572868
  337.3 54.2 %all-gather.17.cloned.1.call-start = ((), (), s32[]{:S(2)}) async-start(), calls=%async_computation.8 | async-start | bytes 2621440 | tf_op jit(solution)/shard_map/all_gather | solution.py:29
  368.9 72.5 %reduce-scatter.5.cloned.1.call-start = ((), (), s32[]{:S(2)}) async-start(), calls=%async_computation.9 | async-start | bytes 2621440 | tf_op jit(solution)/shard_map/reduce_scatter | solution.py:50
  391.6 2.2 copy-start.3
  393.8 3.0 copy-start.6
  398.2 4.7 %collective-permute-start.1 = (bf16[2,512]{1,0:T(2,128)(2,1)S(1)}, bf16[2,512]{1,0:T(2,128)(2,1)S(1)}, u32[]{:S(2)}, u32[]{:S(2)}) collective-permute-start(bf16[2,512]{1,0:T(2,128)(2,1)S(1)} %slice.121), channel_id=1, source_target_pairs={{0,4},{4,8},{8,12},{12,16},{16,20},{20,24},{24,28},{1,5},{5,9},{9,... | collective-permute-start | bytes 6152 | tf_op jit(solution)/shard_map/ppermute | solution.py:13
  409.2 32.2 %copy-start = (bf16[512,512]{1,0:T(8,128)(2,1)S(1)}, bf16[512,512]{1,0:T(8,128)(2,1)}, u32[]{:S(2)}) copy-start(bf16[512,512]{1,0:T(8,128)(2,1)} %add_convert_fusion.1) | copy-start | bytes 1572868
Sparse Core Ops, SparseCore 0:
  8.9 25.2 all-gather.6
  36.4 72.7 all-gather.12
  111.4 71.2 all-gather.10
  184.8 71.2 all-gather.8
  258.0 73.1 all-gather.14
  337.5 29.3 reduce-scatter.2
  369.0 22.5 all-gather.16
  409.3 31.9 reduce-scatter.4
where the time goes:
time: 450 us
  waiting for transfers between devices  399 us (89%)
  matrix products  22.4 us (5%)
  between operations  13.6 us (3%)
  other arithmetic  8.7 us (2%)
  starting transfers between devices  6.12 us (1%)
    all_gather x1, waiting for transfers between devices, on_device(): gathered_out = lax.all_gather(w_output, 'sp', axis=2, tiled=True)  75.1 us
    all_gather x1, waiting for transfers between devices, on_device(): lax.all_gather(w_value, 'sp', axis=1, tiled=True)  72.7 us
    all_gather x1, waiting for transfers between devices, on_device(): lax.all_gather(w_inner, 'sp', axis=1, tiled=True)  70.6 us
    all_gather x1, waiting for transfers between devices, on_device(): lax.all_gather(w_outer, 'sp', axis=1, tiled=True)  66.6 us
    reduce_scatter x2, waiting for transfers between devices, on_device(): lax.psum_scatter(terms.astype(jnp.float32).astype(jnp.bfloat16), 'tp', sc...  61.6 us
    all_gather x2, waiting for transfers between devices, on_device(): full_rows = lax.all_gather(stream_now, 'tp', axis=1, tiled=True)  46.9 us
    dot_general x2, matrix products, on_device(): jnp.dot(gated, layer_output, preferred_element_type=jnp.float32)  12.3 us
  transfers between devices with their start and end apart: 10, of which 10 were waited for; matrix products, arithmetic and copies ran while one was open for 2% of the time, Pallas kernels for 0%

commit v1 on v0

--- a/solution.py
+++ b/solution.py
@@ -26,7 +26,14 @@
         layer_inner = gathered_in[1][layer_index]
         layer_outer = gathered_in[2][layer_index]
         layer_output = gathered_out[layer_index]
-        full_rows = lax.all_gather(stream_now, "tp", axis=1, tiled=True)
+        size = lax.axis_size("tp")
+        hops = [(i_2, (i_2 + 1) % size) for i_2 in range(size)]
+        parts = [stream_now]
+        for far in range(1, size):
+            parts = [lax.ppermute(parts[0], "tp", hops), *parts]
+        out = jnp.concatenate(parts, axis=1)
+        shift = (lax.axis_index("tp") + 1) * parts[-1].shape[1]
+        full_rows = jnp.roll(out, shift, axis=1)
         row_float = full_rows.astype(jnp.float32)
         scale = lax.rsqrt(jnp.mean(row_float * row_float, axis=-1, keepdims=True) + EPSILON)
         normed = (row_float * scale * norm_gain[layer_index]).astype(jnp.bfloat16)

time: 450 us -> 435 us (0.967)
  waiting for transfers between devices: 399 us -> 371 us
  other arithmetic: 8.7 us -> 17.1 us
    ppermute x0 -> x6, waiting for transfers between devices: none -> 51.3 us  [on_device(): parts = [lax.ppermute(parts[0], 'tp', hops), *parts]]
    all_gather x2 -> x0, waiting for transfers between devices: 46.9 us -> none  [on_device(): full_rows = lax.all_gather(stream_now, 'tp', axis=1, tiled=True)]
    all_gather x1, waiting for transfers between devices: 72.7 us -> 43 us  [on_device(): lax.all_gather(w_value, 'sp', axis=1, tiled=True)]
    reduce_sum x2, other arithmetic: 4.45 us -> 11.5 us  [on_device(): jnp.mean(row_float * row_float, axis=-1, keepdims=True) + EPSILON]
  transfers between devices with their start and end apart: 10 -> 14, of which waited for: 10 -> 14; matrix products, arithmetic and copies ran while one was open for 2% -> 3% of each run, Pallas kernels for 0% -> 0%
where the time goes in v1:
time: 435 us; the launch traced here: 434 us
  waiting for transfers between devices  371 us (85%)
  matrix products  23.9 us (5%)
  other arithmetic  17.1 us (4%)
  between operations  13.6 us (3%)
  starting transfers between devices  6.68 us (2%)
    all_gather x1, waiting for transfers between devices, on_device(): gathered_out = lax.all_gather(w_output, 'sp', axis=2, tiled=True)  75.1 us
    all_gather x1, waiting for transfers between devices, on_device(): lax.all_gather(w_inner, 'sp', axis=1, tiled=True)  69.6 us
    all_gather x1, waiting for transfers between devices, on_device(): lax.all_gather(w_outer, 'sp', axis=1, tiled=True)  65.5 us
    reduce_scatter x2, waiting for transfers between devices, on_device(): lax.psum_scatter(terms.astype(jnp.float32).astype(jnp.bfloat16), 'tp', sc...  61.6 us
    ppermute x6, waiting for transfers between devices, on_device(): parts = [lax.ppermute(parts[0], 'tp', hops), *parts]  51.3 us
    all_gather x1, waiting for transfers between devices, on_device(): lax.all_gather(w_value, 'sp', axis=1, tiled=True)  43 us
    dot_general x2, matrix products, on_device(): jnp.dot(gated, layer_output, preferred_element_type=jnp.float32)  14.3 us
    reduce_sum x2, other arithmetic, on_device(): jnp.mean(row_float * row_float, axis=-1, keepdims=True) + EPSILON  11.5 us
  transfers between devices with their start and end apart: 14, of which 14 were waited for; matrix products, arithmetic and copies ran while one was open for 3% of the time, Pallas kernels for 0%

profile of v1, /device:TPU:0, one launch (start us, length us, event | category | flops | bytes accessed | tf_op | source)
XLA Modules:
  0.0 434.2 jit_solution(15407300332681604105)
XLA Ops:
  6.5 0.7 all-gather.9.cloned.1.call-update
  7.3 0.0 all-gather.7.cloned.1.call-start
  7.3 0.7 all-gather.7.cloned.1.call-update
  8.0 0.0 all-gather.5.cloned.1.call-start
  8.1 0.7 all-gather.5.cloned.1.call-update
  8.7 0.0 all-gather.11.cloned.1.call-start
  8.8 0.5 all-gather.11.cloned.1.call-update
  9.3 0.0 reduce-scatter.3.cloned.1.call-start
  9.4 0.5 collective-permute-start
  9.9 9.0 %collective-permute-done = bf16[512,512]{1,0:T(8,128)(2,1)S(1)} collective-permute-done((bf16[512,512]{1,0:T(8,128)(2,1)}, bf16[512,512]{1,0:T(8,128)(2,1)S(1)}, u32[]{:S(2)}, u32[]{:S(2)}) %collective-permute-start) | collective-permute-done | bytes 524320 | tf_op jit(solution)/shard_map/ppermute | solution.py:33
  18.9 0.0 collective-permute-start.1
  19.0 8.6 %collective-permute-done.1 = bf16[512,512]{1,0:T(8,128)(2,1)S(1)} collective-permute-done((bf16[512,512]{1,0:T(8,128)(2,1)S(1)}, bf16[512,512]{1,0:T(8,128)(2,1)S(1)}, u32[]{:S(2)}, u32[]{:S(2)}) %collective-permute-start.1) | collective-permute-done | bytes 524320 | tf_op jit(solution)/shard_map/ppermute | solution.py:33
  27.5 0.0 collective-permute-start.2
  27.5 0.8 fusion.54
  28.4 7.9 %collective-permute-done.2 = bf16[512,512]{1,0:T(8,128)(2,1)} collective-permute-done((bf16[512,512]{1,0:T(8,128)(2,1)S(1)}, bf16[512,512]{1,0:T(8,128)(2,1)}, u32[]{:S(2)}, u32[]{:S(2)}) %collective-permute-start.2) | collective-permute-done | bytes 524320 | tf_op jit(solution)/shard_map/ppermute | solution.py:33
  36.2 5.8 %fusion = (f32[512]{0:T(512)S(1)}, bf16[512,2048]{1,0:T(8,128)(2,1)S(1)}) fusion(s32[]{:T(128)S(6)} %select_n.13, bf16[512,512]{1,0:T(8,128)(2,1)} %param.9, bf16[512,512]{1,0:T(8,128)(2,1)S(1)} %collective-permute-done, bf16[512,512]{1,0:T(8,128)(2,1)S(1)} %collective-permute-done.1, bf16[512,512]{1,0:T(8,128)(2,1)} %collective-permute-done.2), kind=kLoop, calls=%fused_computation.4 | loop fusion | flops 19922432 | bytes 4196356 | tf_op jit(solution)/shard_map/reduce_sum | solution.py:38
  42.1 43.0 %all-gather.9.cloned.1.call-done = bf16[2,2048,512]{2,1,0:T(8,128)(2,1)} async-done(((bf16[2,256,512]{2,1,0:T(8,128)(2,1)}), bf16[2,2048,512]{2,1,0:T(8,128)(2,1)}) %all-gather.9.cloned.1.call-update) | async-done | bytes 4194320 | tf_op jit(solution)/shard_map/all_gather | solution.py:18
  85.0 3.9 fusion.23
  88.9 69.6 %all-gather.7.cloned.1.call-done = bf16[2,2048,512]{2,1,0:T(8,128)(2,1)} async-done(((bf16[2,256,512]{2,1,0:T(8,128)(2,1)}), bf16[2,2048,512]{2,1,0:T(8,128)(2,1)}) %all-gather.7.cloned.1.call-update) | async-done | bytes 4194320 | tf_op jit(solution)/shard_map/all_gather | solution.py:19
  158.6 3.2 fusion.32
  161.7 2.5 collective-permute-start.3
  164.2 1.3 collective-permute-done.3
  165.5 1.1 maximum_convert_fusion
  166.7 65.5 %all-gather.5.cloned.1.call-done = bf16[2,2048,512]{2,1,0:T(8,128)(2,1)} async-done(((bf16[2,256,512]{2,1,0:T(8,128)(2,1)}), bf16[2,2048,512]{2,1,0:T(8,128)(2,1)}) %all-gather.5.cloned.1.call-update) | async-done | bytes 4194320 | tf_op jit(solution)/shard_map/all_gather | solution.py:20
  232.1 75.1 %all-gather.11.cloned.1.call-done = bf16[2,512,2048]{2,1,0:T(8,128)(2,1)} async-done(((bf16[2,512,256]{2,1,0:T(8,128)(2,1)}), bf16[2,512,2048]{2,1,0:T(8,128)(2,1)}) %all-gather.11.cloned.1.call-update) | async-done | bytes 4194320 | tf_op jit(solution)/shard_map/all_gather | solution.py:22
  307.2 7.1 %convolution_convert_fusion.1 = bf16[512,2048]{1,0:T(8,128)(2,1)} fusion(bf16[2,512,2048]{2,1,0:T(8,128)(2,1)} %all-gather.11.cloned.1.call-done, bf16[2,2048,512]{2,1,0:T(8,128)(2,1)} %all-gather.5.cloned.1.call-done, f32[514,512]{1,0:T(8,128)} %maximum_convert_fusion, f32[512]{0:T(512)S(1)} %bitcast.61, f32[512]{0:T(512)S(1)} %bitcast.62, ...), kind=kOutput, calls=%fused_computation.27 | convolution fusion | flops 2154561536 | bytes 11550720 | tf_op jit(solution)/shard_map/dot_general | solution.py:54
  314.3 0.0 reduce-scatter.3.cloned.1.call-update
  314.4 0.0 reduce-scatter.5.cloned.1.call-start
  314.4 29.5 %reduce-scatter.3.cloned.1.call-done = bf16[512,512]{1,0:T(8,128)(2,1)} async-done(((bf16[512,2048]{1,0:T(8,128)(2,1)}), bf16[512,512]{1,0:T(8,128)(2,1)}) %reduce-scatter.3.cloned.1.call-update) | async-done | bytes 524304 | tf_op jit(solution)/shard_map/reduce_scatter | solution.py:57
  343.9 0.0 copy-done
  343.9 1.3 add_convert_fusion.1
  345.2 0.1 collective-permute-start.4
  345.3 8.6 %collective-permute-done.4 = bf16[512,512]{1,0:T(8,128)(2,1)S(1)} collective-permute-done((bf16[512,512]{1,0:T(8,128)(2,1)S(1)}, bf16[512,512]{1,0:T(8,128)(2,1)S(1)}, u32[]{:S(2)}, u32[]{:S(2)}) %collective-permute-start.4) | collective-permute-done | bytes 524320 | tf_op jit(solution)/shard_map/ppermute | solution.py:33
  353.9 0.0 collective-permute-start.5
  353.9 8.6 %collective-permute-done.5 = bf16[512,512]{1,0:T(8,128)(2,1)S(1)} collective-permute-done((bf16[512,512]{1,0:T(8,128)(2,1)S(1)}, bf16[512,512]{1,0:T(8,128)(2,1)S(1)}, u32[]{:S(2)}, u32[]{:S(2)}) %collective-permute-start.5) | collective-permute-done | bytes 524320 | tf_op jit(solution)/shard_map/ppermute | solution.py:33
  362.5 0.0 collective-permute-start.6
  362.5 8.6 %collective-permute-done.6 = bf16[512,512]{1,0:T(8,128)(2,1)S(1)} collective-permute-done((bf16[512,512]{1,0:T(8,128)(2,1)S(1)}, bf16[512,512]{1,0:T(8,128)(2,1)S(1)}, u32[]{:S(2)}, u32[]{:S(2)}) %collective-permute-start.6) | collective-permute-done | bytes 524320 | tf_op jit(solution)/shard_map/ppermute | solution.py:33
  371.1 5.7 %fusion.3 = (f32[512]{0:T(512)S(1)}, bf16[512,2048]{1,0:T(8,128)(2,1)S(1)}) fusion(s32[]{:T(128)S(6)} %select_n.13, bf16[512,512]{1,0:T(8,128)(2,1)S(1)} %add_convert_fusion.1, bf16[512,512]{1,0:T(8,128)(2,1)S(1)} %collective-permute-done.4, bf16[512,512]{1,0:T(8,128)(2,1)S(1)} %collective-permute-done.5, bf16[512,512]{1,0:T(8,128)(2,1)S(1)} %collective-permute-done.6), kind=kLoop, calls=%fused_computation.7 | loop fusion | flops 19922432 | bytes 4196356 | tf_op jit(solution)/shard_map/reduce_sum | solution.py:38
  376.8 1.3 fusion.20
  378.1 0.9 copy-done.3
  379.0 1.3 fusion.30
  380.3 3.4 collective-permute-start.7
  383.7 1.3 collective-permute-done.7
  385.0 1.1 maximum_convert_fusion.1
  386.1 7.2 %convolution_convert_fusion = bf16[512,2048]{1,0:T(8,128)(2,1)} fusion(bf16[2,512,2048]{2,1,0:T(8,128)(2,1)} %all-gather.11.cloned.1.call-done, bf16[2,2048,512]{2,1,0:T(8,128)(2,1)} %all-gather.5.cloned.1.call-done, f32[514,512]{1,0:T(8,128)} %maximum_convert_fusion.1, f32[512]{0:T(512)S(1)} %bitcast.59, f32[512]{0:T(512)S(1)} %bitcast.60, ...), kind=kOutput, calls=%fused_computation.26 | convolution fusion | flops 2154561536 | bytes 11550720 | tf_op jit(solution)/shard_map/dot_general | solution.py:54
  393.3 0.0 reduce-scatter.5.cloned.1.call-update
  393.3 32.1 %reduce-scatter.5.cloned.1.call-done = bf16[512,512]{1,0:T(8,128)(2,1)} async-done(((bf16[512,2048]{1,0:T(8,128)(2,1)}), bf16[512,512]{1,0:T(8,128)(2,1)}) %reduce-scatter.5.cloned.1.call-update) | async-done | bytes 524304 | tf_op jit(solution)/shard_map/reduce_scatter | solution.py:57
  425.4 2.0 add_convert_fusion
  (12 shorter events, 0.1 us)
Async XLA Ops:
  6.5 78.5 %all-gather.9.cloned.1.call-start = ((), (), s32[]{:S(2)}) async-start(), calls=%async_computation.4 | async-start | bytes 4718592 | tf_op jit(solution)/shard_map/all_gather | solution.py:18
  7.3 151.3 %all-gather.7.cloned.1.call-start = ((), (), s32[]{:S(2)}) async-start(), calls=%async_computation.3 | async-start | bytes 4718592 | tf_op jit(solution)/shard_map/all_gather | solution.py:19
  8.0 224.1 %all-gather.5.cloned.1.call-start = ((), (), s32[]{:S(2)}) async-start(), calls=%async_computation.2 | async-start | bytes 4718592 | tf_op jit(solution)/shard_map/all_gather | solution.py:20
  8.7 298.5 %all-gather.11.cloned.1.call-start = ((), (), s32[]{:S(2)}) async-start(), calls=%async_computation.5 | async-start | bytes 4718592 | tf_op jit(solution)/shard_map/all_gather | solution.py:22
  9.3 334.6 %reduce-scatter.3.cloned.1.call-start = ((), (), s32[]{:S(2)}) async-start(), calls=%async_computation.6 | async-start | bytes 2621440 | tf_op jit(solution)/shard_map/reduce_scatter | solution.py:57
  9.4 9.6 %collective-permute-start = (bf16[512,512]{1,0:T(8,128)(2,1)}, bf16[512,512]{1,0:T(8,128)(2,1)S(1)}, u32[]{:S(2)}, u32[]{:S(2)}) collective-permute-start(bf16[512,512]{1,0:T(8,128)(2,1)} %param.9), channel_id=1, source_target_pairs={{0,1},{1,2},{2,3},{3,0},{4,5},{5,6},{6,7},{7,4},{8,9},{9,10},{10,1... | collective-permute-start | bytes 1572872 | tf_op jit(solution)/shard_map/ppermute | solution.py:33
  18.9 8.6 %collective-permute-start.1 = (bf16[512,512]{1,0:T(8,128)(2,1)S(1)}, bf16[512,512]{1,0:T(8,128)(2,1)S(1)}, u32[]{:S(2)}, u32[]{:S(2)}) collective-permute-start(bf16[512,512]{1,0:T(8,128)(2,1)S(1)} %collective-permute-done), channel_id=1, source_target_pairs={{0,1},{1,2},{2,3},{3,0},{4,5},{5,6},{6,7},{7,4},{8,9},{9,10},{10,1... | collective-permute-start | bytes 1572872 | tf_op jit(solution)/shard_map/ppermute | solution.py:33
  27.5 8.7 %collective-permute-start.2 = (bf16[512,512]{1,0:T(8,128)(2,1)S(1)}, bf16[512,512]{1,0:T(8,128)(2,1)}, u32[]{:S(2)}, u32[]{:S(2)}) collective-permute-start(bf16[512,512]{1,0:T(8,128)(2,1)S(1)} %collective-permute-done.1), channel_id=1, source_target_pairs={{0,1},{1,2},{2,3},{3,0},{4,5},{5,6},{6,7},{7,4},{8,9},{9,10},{10,1... | collective-permute-start | bytes 1572872 | tf_op jit(solution)/shard_map/ppermute | solution.py:33
  88.9 75.3 %copy-start.1 = (f32[2,3,512]{2,0,1:T(2,128)S(1)}, f32[2,3,512]{2,0,1:T(2,128)}, u32[]{:S(2)}) copy-start(f32[2,3,512]{2,0,1:T(2,128)} %param.14) | copy-start | bytes 36868
  161.7 3.8 collective-permute-start.3
  307.2 36.7 %copy-start = (bf16[512,512]{1,0:T(8,128)(2,1)S(1)}, bf16[512,512]{1,0:T(8,128)(2,1)}, u32[]{:S(2)}) copy-start(bf16[512,512]{1,0:T(8,128)(2,1)} %param.9) | copy-start | bytes 1572868
  314.4 111.1 %reduce-scatter.5.cloned.1.call-start = ((), (), s32[]{:S(2)}) async-start(), calls=%async_computation.7 | async-start | bytes 2621440 | tf_op jit(solution)/shard_map/reduce_scatter | solution.py:57
  343.9 32.9 %copy-start.2 = (bf16[2,2048,512]{2,1,0:T(8,128)(2,1)S(1)}, bf16[2,2048,512]{2,1,0:T(8,128)(2,1)}, u32[]{:S(2)}) copy-start(bf16[2,2048,512]{2,1,0:T(8,128)(2,1)} %all-gather.9.cloned.1.call-done) | copy-start | bytes 12582916
  345.2 8.7 %collective-permute-start.4 = (bf16[512,512]{1,0:T(8,128)(2,1)S(1)}, bf16[512,512]{1,0:T(8,128)(2,1)S(1)}, u32[]{:S(2)}, u32[]{:S(2)}) collective-permute-start(bf16[512,512]{1,0:T(8,128)(2,1)S(1)} %add_convert_fusion.1), channel_id=1, source_target_pairs={{0,1},{1,2},{2,3},{3,0},{4,5},{5,6},{6,7},{7,4},{8,9},{9,10},{10,1... | collective-permute-start | bytes 1572872 | tf_op jit(solution)/shard_map/ppermute | solution.py:33
  353.9 8.6 %collective-permute-start.5 = (bf16[512,512]{1,0:T(8,128)(2,1)S(1)}, bf16[512,512]{1,0:T(8,128)(2,1)S(1)}, u32[]{:S(2)}, u32[]{:S(2)}) collective-permute-start(bf16[512,512]{1,0:T(8,128)(2,1)S(1)} %collective-permute-done.4), channel_id=1, source_target_pairs={{0,1},{1,2},{2,3},{3,0},{4,5},{5,6},{6,7},{7,4},{8,9},{9,10},{10,1... | collective-permute-start | bytes 1572872 | tf_op jit(solution)/shard_map/ppermute | solution.py:33
  362.5 8.6 %collective-permute-start.6 = (bf16[512,512]{1,0:T(8,128)(2,1)S(1)}, bf16[512,512]{1,0:T(8,128)(2,1)S(1)}, u32[]{:S(2)}, u32[]{:S(2)}) collective-permute-start(bf16[512,512]{1,0:T(8,128)(2,1)S(1)} %collective-permute-done.5), channel_id=1, source_target_pairs={{0,1},{1,2},{2,3},{3,0},{4,5},{5,6},{6,7},{7,4},{8,9},{9,10},{10,1... | collective-permute-start | bytes 1572872 | tf_op jit(solution)/shard_map/ppermute | solution.py:33
  376.8 2.2 copy-start.3
  380.3 4.7 %collective-permute-start.7 = (bf16[2,512]{1,0:T(2,128)(2,1)S(1)}, bf16[2,512]{1,0:T(2,128)(2,1)S(1)}, u32[]{:S(2)}, u32[]{:S(2)}) collective-permute-start(bf16[2,512]{1,0:T(2,128)(2,1)S(1)} %slice.121), channel_id=1, source_target_pairs={{0,4},{4,8},{8,12},{12,16},{16,20},{20,24},{24,28},{1,5},{5,9},{9,... | collective-permute-start | bytes 6152 | tf_op jit(solution)/shard_map/ppermute | solution.py:13
Sparse Core Ops, SparseCore 0:
  9.5 75.4 all-gather.8
  87.2 71.2 all-gather.6
  160.8 71.2 all-gather.4
  234.0 73.1 all-gather.10
  314.5 29.3 reduce-scatter.2
  393.4 31.9 reduce-scatter.4
